TPU v7x, 32 devices: a whole 2x2x4 slice. The times are simulated.
32 devices in a mesh: fs: 8 (over z, x), tp: 4 (over y, core).
Axes of the slice: x: 2, y: 2, z: 4, core: 2. Of those that a mesh axis runs over, the one named last changes fastest.
Arguments:
- saved_input: bfloat16 [20480, 2048], P('fs'), may hold values from -6 to 6
- value_cot: bfloat16 [20480, 1024], P('fs', 'tp'), may hold values from -6 to 6
- query_cot: bfloat16 [20480, 512], P('fs', 'tp'), may hold values from -6 to 6
- value_master: float32 [2048, 1024], P('fs', 'tp'), may hold values from -0.125 to 0.125
- query_master: float32 [2048, 512], P('fs', 'tp'), may hold values from -0.125 to 0.125
- value_factor: bfloat16 [2048, 256], P('fs'), may hold values from -0.125 to 0.125
- query_factor: bfloat16 [2048, 256], P('fs'), may hold values from -0.125 to 0.125
- value_first: float32 [256, 1024], P('fs', 'tp'), as said below
- value_second: float32 [256, 1024], P('fs', 'tp'), as said below
- query_first: float32 [256, 512], P('fs', 'tp'), as said below
- query_second: float32 [256, 512], P('fs', 'tp'), as said below
Outputs:
- value_step: float32 [2048, 1024], P('fs', 'tp')
- query_step: float32 [2048, 512], P('fs', 'tp')
- value_master_new: float32 [2048, 1024], P('fs', 'tp')
- query_master_new: float32 [2048, 512], P('fs', 'tp')
- value_copy: bfloat16 [2048, 1024], P(None, 'tp')
- query_copy: bfloat16 [2048, 512], P(None, 'tp')
- value_first_new: float32 [256, 1024], P('fs', 'tp')
- value_second_new: float32 [256, 1024], P('fs', 'tp')
- query_first_new: float32 [256, 512], P('fs', 'tp')
- query_second_new: float32 [256, 512], P('fs', 'tp')
Inputs may be any that keep to these rules, and one draw needn't show every extreme that they name: `value_first`: first moments are real-valued of the projected gradient's order. `value_second`: second moments are positive. `query_first`: first moments are real-valued of the projected gradient's order. `query_second`: second moments are positive.
All inputs are finite; a program needn't handle non-finite values.
Results may differ from a plain program's by a relative error of at most 0.001.
Values may be sent and summed in bfloat16 or wider, within the bound.
A program may use at most 64 MiB of HBM per device.

v0:
```python
import jax
import jax.numpy as jnp
from jax import lax
from jax.sharding import PartitionSpec as P

RANK = 256
V_W = 1024
QK_W = 512


BETA_ONE = 0.9
BETA_TWO = 0.95
DENOM_EPS = 1e-08
NORM_EPS = 1e-06
STEP_SIZE = 0.05


def moment_update(projected, first, second):
    first_new = BETA_ONE * first + (1.0 - BETA_ONE) * projected
    second_new = BETA_TWO * second + (1.0 - BETA_TWO) * projected * projected
    direction = first_new / (jnp.sqrt(second_new) + DENOM_EPS)
    return (first_new, second_new, direction)


def on_device(
    saved_input,
    value_cot,
    query_cot,
    value_master,
    query_master,
    value_factor,
    query_factor,
    value_first,
    value_second,
    query_first,
    query_second,
):
    shards = lax.axis_size("fs")
    tokens_all = saved_input.shape[0] * shards
    highest = lax.Precision.HIGHEST
    value_reduced = jnp.dot(
        saved_input,
        lax.all_gather(value_factor, "fs", axis=0, tiled=True),
        preferred_element_type=jnp.float32,
    )
    query_reduced = jnp.dot(
        saved_input,
        lax.all_gather(query_factor, "fs", axis=0, tiled=True),
        preferred_element_type=jnp.float32,
    )
    value_part = (
        lax.dot_general(
            value_reduced,
            value_cot.astype(jnp.float32),
            (((0,), (0,)), ((), ())),
            precision=highest,
        )
        / tokens_all
    )
    query_part = (
        lax.dot_general(
            query_reduced,
            query_cot.astype(jnp.float32),
            (((0,), (0,)), ((), ())),
            precision=highest,
        )
        / tokens_all
    )
    value_share, query_share = (
        lax.psum_scatter(value_part, "fs", scatter_dimension=0, tiled=True),
        lax.psum_scatter(query_part, "fs", scatter_dimension=0, tiled=True),
    )
    value_first_new, value_second_new, value_dir_own = moment_update(
        value_share, value_first, value_second
    )
    query_first_new, query_second_new, query_dir_own = moment_update(
        query_share, query_first, query_second
    )
    value_direction, query_direction = (
        lax.all_gather(value_dir_own, "fs", axis=0, tiled=True),
        lax.all_gather(query_dir_own, "fs", axis=0, tiled=True),
    )
    square_sum = lax.psum(
        jnp.sum(value_dir_own * value_dir_own) + jnp.sum(query_dir_own * query_dir_own),
        ("fs", "tp"),
    )
    update_scale = 1.0 / jnp.sqrt(square_sum / (RANK * (V_W + QK_W)) + NORM_EPS)
    value_step = (
        jnp.dot(value_factor.astype(jnp.float32), value_direction, precision=highest) * update_scale
    )
    query_step = (
        jnp.dot(query_factor.astype(jnp.float32), query_direction, precision=highest) * update_scale
    )
    value_master_new = value_master - STEP_SIZE * value_step
    query_master_new = query_master - STEP_SIZE * query_step
    value_copy, query_copy = (
        lax.all_gather(value_master_new.astype(jnp.bfloat16), "fs", axis=0, tiled=True),
        lax.all_gather(query_master_new.astype(jnp.bfloat16), "fs", axis=0, tiled=True),
    )
    return (
        value_step,
        query_step,
        value_master_new,
        query_master_new,
        value_copy,
        query_copy,
        value_first_new,
        value_second_new,
        query_first_new,
        query_second_new,
    )


def solution(mesh):
    in_specs = (
        P("fs", None),
        P("fs", "tp"),
        P("fs", "tp"),
        P("fs", "tp"),
        P("fs", "tp"),
        P("fs", None),
        P("fs", None),
        P("fs", "tp"),
        P("fs", "tp"),
        P("fs", "tp"),
        P("fs", "tp"),
    )
    out_specs = (
        P("fs", "tp"),
        P("fs", "tp"),
        P("fs", "tp"),
        P("fs", "tp"),
        P(None, "tp"),
        P(None, "tp"),
        P("fs", "tp"),
        P("fs", "tp"),
        P("fs", "tp"),
        P("fs", "tp"),
    )
    return jax.shard_map(
        on_device, mesh=mesh, in_specs=in_specs, out_specs=out_specs, check_vma=False
    )
```

profile of v0, /device:TPU:0, one launch (start us, length us, event | category | flops | bytes accessed | tf_op | source)
XLA Modules:
  0.0 375.6 jit_solution(1386011810459708542)
XLA Ops:
  7.2 0.0 copy-start
  7.2 0.0 all-gather.6.cloned.1.call-start
  7.2 0.7 all-gather.6.cloned.1.call-update
  7.9 0.0 all-gather.4.cloned.1.call-start
  8.0 0.7 all-gather.4.cloned.1.call-update
  8.7 0.0 copy-start.1
  8.7 0.0 reduce-scatter.5.cloned.1.call-start
  8.7 44.4 %all-gather.6.cloned.1.call-done = bf16[2048,256]{1,0:T(8,128)(2,1)} async-done(((bf16[256,256]{1,0:T(8,128)(2,1)}), bf16[2048,256]{1,0:T(8,128)(2,1)}) %all-gather.6.cloned.1.call-update) | async-done | bytes 1048592 | tf_op jit(solution)/shard_map/all_gather | solution.py:48
  53.2 5.9 %fusion.9 = f32[2560,256]{1,0:T(8,128)S(1)} fusion(bf16[2560,2048]{1,0:T(8,128)(2,1)} %param.11, bf16[2048,256]{1,0:T(8,128)(2,1)} %all-gather.6.cloned.1.call-done), kind=kOutput, calls=%fused_computation.21 | convolution fusion | flops 2684354560 | bytes 14155776 | tf_op jit(solution)/shard_map/dot_general | solution.py:46
  59.1 0.0 copy-done.1
  59.1 2.9 convolution_multiply_fusion.3
  61.9 0.0 reduce-scatter.5.cloned.1.call-update
  62.0 0.0 reduce-scatter.3.cloned.1.call-start
  62.0 32.3 %all-gather.4.cloned.1.call-done = bf16[2048,256]{1,0:T(8,128)(2,1)} async-done(((bf16[256,256]{1,0:T(8,128)(2,1)}), bf16[2048,256]{1,0:T(8,128)(2,1)}) %all-gather.4.cloned.1.call-update) | async-done | bytes 1048592 | tf_op jit(solution)/shard_map/all_gather | solution.py:43
  94.3 5.9 %fusion.8 = f32[2560,256]{1,0:T(8,128)S(1)} fusion(bf16[2560,2048]{1,0:T(8,128)(2,1)} %param.11, bf16[2048,256]{1,0:T(8,128)(2,1)} %all-gather.4.cloned.1.call-done), kind=kOutput, calls=%fused_computation.20 | convolution fusion | flops 2684354560 | bytes 14155776 | tf_op jit(solution)/shard_map/dot_general | solution.py:41
  100.2 0.0 copy-done
  100.2 0.0 copy-start.8
  100.2 0.0 copy-start.9
  100.2 0.0 copy-start.6
  100.3 0.0 copy-start.7
  100.3 0.0 copy-start.4
  100.3 0.0 copy-start.2
  100.3 0.0 copy-start.5
  100.3 2.9 convolution_multiply_fusion.1
  103.2 0.0 reduce-scatter.3.cloned.1.call-update
  103.3 0.0 all-gather.8.cloned.1.call-start
  103.3 55.4 %reduce-scatter.5.cloned.1.call-done = f32[32,128]{1,0:T(8,128)} async-done(((f32[256,128]{1,0:T(8,128)}), f32[32,128]{1,0:T(8,128)}) %reduce-scatter.5.cloned.1.call-update) | async-done | bytes 16400 | tf_op jit(solution)/shard_map/reduce_scatter | solution.py:71
  158.7 0.0 copy-done.8
  158.7 1.9 multiply_reduce_fusion.1
  160.7 63.0 %reduce-scatter.3.cloned.1.call-done = f32[32,256]{1,0:T(8,128)} async-done(((f32[256,256]{1,0:T(8,128)}), f32[32,256]{1,0:T(8,128)}) %reduce-scatter.3.cloned.1.call-update) | async-done | bytes 32784 | tf_op jit(solution)/shard_map/reduce_scatter | solution.py:70
  223.6 0.0 copy-done.7
  223.6 2.0 multiply_reduce_fusion
  226.9 0.1 copy.21
  227.1 40.1 %psum.7 = f32[]{:T(128)} all-reduce(f32[]{:T(128)S(6)} %add.44), channel_id=1, replica_groups=mesh['fs'=8,'tp'=4] {'fs','tp'}, use_global_device_ids=true, to_apply=%region_4.0 | all-reduce | flops 1 | bytes 8 | tf_op jit(solution)/shard_map/psum | solution.py:83
  267.9 30.8 %all_gather.19 = f32[256,256]{1,0:T(8,128)S(1)} all-gather(f32[32,256]{1,0:T(8,128)S(1)} %get-tuple-element.29), channel_id=1, replica_groups=mesh['fs'=8,'tp'=4] {'fs'}, dimensions={0}, use_global_device_ids=true | all-gather | bytes 294912 | tf_op jit(solution)/shard_map/all_gather | solution.py:80
  298.7 0.0 copy-done.2
  298.7 1.1 fusion.5
  299.7 0.0 all-gather.8.cloned.1.call-update
  299.7 0.1 copy.22
  299.8 30.9 %all_gather.21 = f32[256,128]{1,0:T(8,128)S(1)} all-gather(f32[32,128]{1,0:T(8,128)S(1)} %get-tuple-element.25), channel_id=1, replica_groups=mesh['fs'=8,'tp'=4] {'fs'}, dimensions={0}, use_global_device_ids=true | all-gather | bytes 147456 | tf_op jit(solution)/shard_map/all_gather | solution.py:81
  330.8 0.3 fusion.4
  331.1 31.5 %all_gather.23 = bf16[2048,128]{0,1:T(8,128)(2,1)S(1)} all-gather(bf16[256,128]{0,1:T(8,128)(2,1)S(1)} %get-tuple-element.20), channel_id=1, replica_groups=mesh['fs'=8,'tp'=4] {'fs'}, dimensions={0}, use_global_device_ids=true | all-gather | bytes 589824 | tf_op jit(solution)/shard_map/all_gather | solution.py:98
  362.6 1.0 copy.28
  363.6 0.8 copy.24
  364.4 0.8 copy.26
  365.1 0.8 copy.23
  366.0 0.8 copy.25
  366.8 2.3 copy.27
  (7 shorter events, 0.0 us)
Async XLA Ops:
  7.2 93.0 %copy-start = (bf16[2560,256]{1,0:T(8,128)(2,1)S(1)}, bf16[2560,256]{1,0:T(8,128)(2,1)}, u32[]{:S(2)}) copy-start(bf16[2560,256]{1,0:T(8,128)(2,1)} %param.12) | copy-start | bytes 3932164
  7.2 46.0 %all-gather.6.cloned.1.call-start = ((), (), s32[]{:S(2)}) async-start(), calls=%async_computation.4 | async-start | bytes 1179648 | tf_op jit(solution)/shard_map/all_gather | solution.py:48
  7.9 86.4 %all-gather.4.cloned.1.call-start = ((), (), s32[]{:S(2)}) async-start(), calls=%async_computation.2 | async-start | bytes 1179648 | tf_op jit(solution)/shard_map/all_gather | solution.py:43
  8.7 50.4 %copy-start.1 = (bf16[2560,128]{1,0:T(8,128)(2,1)S(1)}, bf16[2560,128]{1,0:T(8,128)(2,1)}, u32[]{:S(2)}) copy-start(bf16[2560,128]{1,0:T(8,128)(2,1)} %param.13) | copy-start | bytes 1966084
  8.7 150.0 %reduce-scatter.5.cloned.1.call-start = ((), (), s32[]{:S(2)}) async-start(), calls=%async_computation.5 | async-start | bytes 147456 | tf_op jit(solution)/shard_map/reduce_scatter | solution.py:71
  62.0 161.7 %reduce-scatter.3.cloned.1.call-start = ((), (), s32[]{:S(2)}) async-start(), calls=%async_computation.3 | async-start | bytes 294912 | tf_op jit(solution)/shard_map/reduce_scatter | solution.py:70
  100.2 58.5 %copy-start.8 = (f32[32,128]{1,0:T(8,128)S(1)}, f32[32,128]{1,0:T(8,128)}, u32[]{:S(2)}) copy-start(f32[32,128]{1,0:T(8,128)} %param.21) | copy-start | bytes 49156
  100.2 58.5 %copy-start.9 = (f32[32,128]{1,0:T(8,128)S(1)}, f32[32,128]{1,0:T(8,128)}, u32[]{:S(2)}) copy-start(f32[32,128]{1,0:T(8,128)} %param.20) | copy-start | bytes 49156
  100.2 123.4 %copy-start.6 = (f32[32,256]{1,0:T(8,128)S(1)}, f32[32,256]{1,0:T(8,128)}, u32[]{:S(2)}) copy-start(f32[32,256]{1,0:T(8,128)} %param.19) | copy-start | bytes 98308
  100.3 123.4 %copy-start.7 = (f32[32,256]{1,0:T(8,128)S(1)}, f32[32,256]{1,0:T(8,128)}, u32[]{:S(2)}) copy-start(f32[32,256]{1,0:T(8,128)} %param.18) | copy-start | bytes 98308
  100.3 126.6 %copy-start.4 = (f32[256,256]{1,0:T(8,128)S(1)}, f32[256,256]{1,0:T(8,128)}, u32[]{:S(2)}) copy-start(f32[256,256]{1,0:T(8,128)} %param.14) | copy-start | bytes 786436
  100.3 198.4 %copy-start.2 = (bf16[256,256]{1,0:T(8,128)(2,1)S(1)}, bf16[256,256]{1,0:T(8,128)(2,1)}, u32[]{:S(2)}) copy-start(bf16[256,256]{1,0:T(8,128)(2,1)} %param.16) | copy-start | bytes 393220
  100.3 199.4 %copy-start.5 = (f32[256,128]{1,0:T(8,128)S(1)}, f32[256,128]{1,0:T(8,128)}, u32[]{:S(2)}) copy-start(f32[256,128]{1,0:T(8,128)} %param.15) | copy-start | bytes 393220
  103.2 227.6 %copy-start.3 = (bf16[256,256]{1,0:T(8,128)(2,1)S(1)}, bf16[256,256]{1,0:T(8,128)(2,1)}, u32[]{:S(2)}) copy-start(bf16[256,256]{1,0:T(8,128)(2,1)} %param.17) | copy-start | bytes 393220
  103.3 263.5 %all-gather.8.cloned.1.call-start = ((), (), s32[]{:S(2)}) async-start(), calls=%async_computation.6 | async-start | bytes 1179648 | tf_op jit(solution)/shard_map/all_gather | solution.py:97
Sparse Core Ops, SparseCore 0:
  10.1 42.9 all-gather.5
  55.3 38.9 all-gather.3
  98.2 60.4 reduce-scatter.4
  162.5 61.0 reduce-scatter.2
  299.9 40.3 all-gather.7
where the time goes:
time: 376 us
  waiting for transfers between devices  197 us (52%)
  blocking collectives  133 us (35%)
  matrix products  19 us (5%)
  between operations  15.9 us (4%)
  local copies, waits for them, and re-layouts  6.72 us (2%)
  other arithmetic  3.92 us (1%)
    reduce_scatter x1, waiting for transfers between devices, on_device(): lax.psum_scatter(value_part, 'fs', scatter_dimension=0, tiled=True)  63 us
    reduce_scatter x1, waiting for transfers between devices, on_device(): lax.psum_scatter(query_part, 'fs', scatter_dimension=0, tiled=True)  55.4 us
    all_gather x1, waiting for transfers between devices, on_device(): lax.all_gather(query_factor, 'fs', axis=0, tiled=True)  44.4 us
    psum x1, blocking collectives, on_device(): lax.psum(jnp.sum(value_dir_own * value_dir_own) + jnp.sum(query_dir_own *...  40.1 us
    all_gather x1, waiting for transfers between devices, on_device(): lax.all_gather(value_factor, 'fs', axis=0, tiled=True)  32.3 us
    all_gather x1, blocking collectives, on_device(): lax.all_gather(query_master_new.astype(jnp.bfloat16), 'fs', axis=0, tiled...  31.5 us
    all_gather x1, blocking collectives, on_device(): lax.all_gather(query_dir_own, 'fs', axis=0, tiled=True)  30.9 us
    all_gather x1, blocking collectives, on_device(): lax.all_gather(value_dir_own, 'fs', axis=0, tiled=True)  30.8 us
  transfers between devices with their start and end apart: 5, of which 4 were waited for; matrix products, arithmetic and copies ran while one was open for 6% of the time, Pallas kernels for 0%

commit v1 on v0

v1 whole, which is shorter than its diff:
```python
import functools

import jax
import jax.numpy as jnp
from jax import lax
from jax.experimental import pallas as pl
from jax.experimental.pallas import tpu as pltpu
from jax.sharding import PartitionSpec as P

BETA_ONE = 0.9
BETA_TWO = 0.95
DENOM_EPS = 1e-08
NORM_EPS = 1e-06
STEP_SIZE = 0.05

MESH = pl.DeviceIdType.MESH
F32 = jnp.float32
BF16 = jnp.bfloat16


def split_dot(lhs, rhs):
    return jnp.dot(lhs, rhs, preferred_element_type=F32)


class Gather:
    def __init__(self, slot, parts, nz, nx, me, send_sem, recv_sem, extra=None):
        self.slot, self.parts, self.nz, self.nx = slot, parts, nz, nx
        self.me, self.z, self.x = me, me // nx, me % nx
        self.send_sem, self.recv_sem, self.extra = send_sem, recv_sem, extra
        self.sent = []

    def copy(self, part, index, kind, peer):
        ref = self.slot(index, part)
        return pltpu.make_async_remote_copy(
            src_ref=ref,
            dst_ref=ref,
            send_sem=self.send_sem.at[part, index, kind],
            recv_sem=self.recv_sem.at[part, index],
            device_id={"fs": peer},
            device_id_type=MESH,
        )

    def send(self, part, index, kind, peer, where):
        def go():
            self.copy(part, index, kind, peer).start()

        def done():
            self.copy(part, index, kind, peer).wait_send()

        pl.when(where)(go)
        self.sent.append((where, done))

    def up(self, part, index, where):
        self.send(part, index, 0, jnp.minimum(self.me + self.nx, self.nz * self.nx - 1),
                  jnp.logical_and(where, self.z < self.nz - 1))

    def down(self, part, index, where):
        self.send(part, index, 1, jnp.maximum(self.me - self.nx, 0), jnp.logical_and(where, self.z > 0))

    def across(self, part, index, where):
        for k in range(1, self.nx):
            peer = self.z * self.nx + (self.x + k) % self.nx
            self.send(part, index, 1 + k, peer, where)

    def arrived(self, part, index, where):
        def go():
            self.copy(part, index, 0, self.me).wait_recv()
            if self.extra is not None:
                self.extra(part, index)

        pl.when(where)(go)

    def start(self):
        yes = self.z >= 0
        for part in range(self.parts):
            if part == 1:
                self.across(part, self.me, yes)
            self.up(part, self.me, yes)
            self.down(part, self.me, yes)
            if part == 0:
                self.across(part, self.me, yes)

    def side(self):
        yes = self.z >= 0
        for k in range(1, self.nx):
            index = self.z * self.nx + (self.x + k) % self.nx
            if self.parts > 1:
                self.arrived(1, index, yes)
                self.up(1, index, yes)
                self.down(1, index, yes)

    def hop(self, s):
        below, above = self.z >= s, self.z + s < self.nz
        low = jnp.maximum(self.z - s, 0) * self.nx
        high = jnp.minimum(self.z + s, self.nz - 1) * self.nx
        for where, base, onward in ((below, low, self.up), (above, high, self.down)):
            index = base + self.x
            self.arrived(0, index, where)
            onward(0, index, where)
            self.across(0, index, where)
            if self.parts > 1:
                for k in range(self.nx):
                    index = base + (self.x + k) % self.nx
                    self.arrived(1, index, where)
                    onward(1, index, where)

    def last(self):
        yes = self.z >= 0
        for z in range(self.nz):
            for k in range(1, self.nx):
                self.arrived(0, z * self.nx + (self.x + k) % self.nx, yes)

    def drain(self):
        for where, done in self.sent:
            pl.when(where)(done)

    def whole(self):
        self.start()
        self.side()
        for s in range(1, self.nz):
            self.hop(s)
        self.last()


def kernel(
    nfs, ntp, nz, nx, total_tokens, entries,
    x_in, cv_in, cq_in, mv_in, mq_in, fv_in, fq_in, v1_in, v2_in, q1_in, q2_in,
    step_v, step_q, new_v, new_q, copy_v, copy_q, v1, v2, q1, q2,
    xs, cv, cq, ct, gh, gl, fac, part, landed, dirs, sums, cop, mv, mq, m1v, m2v, m1q, m2q,
    load_sem, x_sem, fsend, frecv, sib_send, sib_recv, dsend, drecv, csend, crecv, rs_sem, sum_sem,
):
    me, tp = lax.axis_index("fs"), lax.axis_index("tp")
    core, sibling = tp % 2, tp + 1 - 2 * (tp % 2)
    blocks, tokens, width = xs.shape
    rows, rank = fv_in.shape
    wv, wq = cv.shape[1], cq.shape[1]
    rk = v1_in.shape[0]
    fparts, fhalf = fac.shape[2], fac.shape[3]
    dparts, dhalf = dirs.shape[1], dirs.shape[2]
    cparts, chalf = cop.shape[1], cop.shape[2]

    loads = []

    def load(src, dst):
        copy = pltpu.make_async_copy(src, dst, load_sem.at[len(loads)])
        copy.start()
        loads.append(copy)

    for p in range(fparts):
        load(fv_in.at[pl.ds(p * fhalf, fhalf)], fac.at[0, me, p])
        load(fq_in.at[pl.ds(p * fhalf, fhalf)], fac.at[1, me, p])
    nfac = len(loads)
    load(cv_in, cv)
    load(cq_in, cq)
    xcopies = []
    for b in range(blocks):
        copy = pltpu.make_async_copy(x_in.at[:, pl.ds(b * width, width)], xs.at[b], x_sem.at[b])
        copy.start()
        xcopies.append(copy)
    for src, dst in ((v1_in, m1v), (v2_in, m2v), (q1_in, m1q), (q2_in, m2q), (mv_in, mv), (mq_in, mq)):
        load(src, dst)

    barrier = pltpu.get_barrier_semaphore()
    devices = nfs * ntp
    mine = me * ntp + tp

    def greet(k, _):
        other = (mine + k) % devices
        pl.semaphore_signal(
            barrier, inc=1, device_id={"fs": other // ntp, "tp": other % ntp}, device_id_type=MESH
        )
        return 0

    lax.fori_loop(1, devices, greet, 0)
    for copy in loads[:nfac]:
        copy.wait()
    pl.semaphore_wait(barrier, devices - 1)

    def to_sibling(p, index):
        return pltpu.make_async_remote_copy(
            src_ref=fac.at[core, index, p],
            dst_ref=fac.at[core, index, p],
            send_sem=sib_send.at[p, index],
            recv_sem=sib_recv.at[p, index],
            device_id={"tp": sibling},
            device_id_type=MESH,
        )

    factors = Gather(
        lambda index, p: fac.at[core, index, p], fparts, nz, nx, me, fsend, frecv,
        extra=lambda p, index: to_sibling(p, index).start(),
    )
    factors.start()

    loads[nfac].wait()
    loads[nfac + 1].wait()
    ct[0:wv, :] = cv[...].T
    ct[wv : wv + wq, :] = cq[...].T
    inverse = 1.0 / total_tokens

    def grad_block(b):
        xcopies[b].wait()
        g = split_dot(ct[...], xs[b]) * inverse
        high = g.astype(BF16)
        gh[b] = high
        gl[b] = (g - high.astype(F32)).astype(BF16)

    todo = [factors.side] + [functools.partial(factors.hop, s) for s in range(1, nz)]
    for b in range(blocks):
        grad_block(b)
        if b < len(todo):
            todo[b]()
    for work in todo[blocks:]:
        work()
    factors.last()
    for p in range(fparts):
        for k in range(1, nfs):
            index = (me + k) % nfs
            pltpu.make_async_remote_copy(
                src_ref=fac.at[1 - core, index, p],
                dst_ref=fac.at[1 - core, index, p],
                send_sem=sib_send.at[p, index],
                recv_sem=sib_recv.at[p, index],
                device_id={"tp": sibling},
                device_id_type=MESH,
            ).wait_recv()

    all_v = fac[0].reshape(blocks, width, rank)
    all_q = fac[1].reshape(blocks, width, rank)
    acc_v = jnp.zeros((wv, rank), F32)
    acc_q = jnp.zeros((wq, rank), F32)
    for b in range(blocks):
        for g in (gl, gh):
            acc_v += split_dot(g[b, 0:wv, :], all_v[b])
            acc_q += split_dot(g[b, wv : wv + wq, :], all_q[b])
    part[:, :, 0:wv] = acc_v.T.reshape(nfs, rk, wv)
    part[:, :, wv : wv + wq] = acc_q.T.reshape(nfs, rk, wq)

    for k in range(1, nfs):
        peer = (me + k) % nfs
        pltpu.make_async_remote_copy(
            src_ref=part.at[peer],
            dst_ref=landed.at[k - 1],
            send_sem=rs_sem.at[0],
            recv_sem=rs_sem.at[1],
            device_id={"fs": peer},
            device_id_type=MESH,
        ).start()
    for copy in loads[nfac + 2 :]:
        copy.wait()
    everything = pltpu.make_async_remote_copy(
        src_ref=landed,
        dst_ref=landed,
        send_sem=rs_sem.at[0],
        recv_sem=rs_sem.at[1],
        device_id={"fs": me},
        device_id_type=MESH,
    )
    everything.wait_recv()
    share = part[me]
    for k in range(nfs - 1):
        share = share + landed[k]

    square = jnp.zeros((), F32)
    for cols, first_ref, second_ref, first_out, second_out in (
        (slice(0, wv), m1v, m2v, v1, v2),
        (slice(wv, wv + wq), m1q, m2q, q1, q2),
    ):
        projected = share[:, cols]
        first_new = BETA_ONE * first_ref[...] + (1.0 - BETA_ONE) * projected
        second_new = BETA_TWO * second_ref[...] + (1.0 - BETA_TWO) * projected * projected
        first_out[...] = first_new
        second_out[...] = second_new
        direction = first_new / (jnp.sqrt(second_new) + DENOM_EPS)
        dirs[me, :, :, cols] = direction.reshape(dparts, dhalf, direction.shape[1])
        square = square + jnp.sum(direction * direction)
    sums[devices - 1] = jnp.full(sums.shape[1:], square, F32)

    directions = Gather(lambda index, p: dirs.at[index, p], dparts, nz, nx, me, dsend, drecv)
    directions.start()

    def tell(k, _):
        other = (mine + k) % devices
        pltpu.make_async_remote_copy(
            src_ref=sums.at[devices - 1],
            dst_ref=sums.at[devices - 1 - k],
            send_sem=sum_sem.at[0],
            recv_sem=sum_sem.at[1],
            device_id={"fs": other // ntp, "tp": other % ntp},
            device_id_type=MESH,
        ).start()
        return 0

    lax.fori_loop(1, devices, tell, 0)
    directions.side()
    for s in range(1, nz):
        directions.hop(s)
    directions.last()

    full = dirs[...].reshape(rank, wv + wq)
    high = full.astype(BF16)
    low = (full - high.astype(F32)).astype(BF16)
    own_v = fac[0, me].reshape(rows, rank)
    own_q = fac[1, me].reshape(rows, rank)
    raw_v = split_dot(own_v, low[:, 0:wv]) + split_dot(own_v, high[:, 0:wv])
    raw_q = split_dot(own_q, low[:, wv:]) + split_dot(own_q, high[:, wv:])

    told = pltpu.make_async_remote_copy(
        src_ref=sums.at[pl.ds(0, devices - 1)],
        dst_ref=sums.at[pl.ds(0, devices - 1)],
        send_sem=sum_sem.at[0],
        recv_sem=sum_sem.at[1],
        device_id={"fs": me},
        device_id_type=MESH,
    )
    told.wait_recv()
    square_sum = jnp.sum(sums[...], axis=0)[0:1, 0:1]
    scale = 1.0 / jnp.sqrt(square_sum / entries + NORM_EPS)
    sv = raw_v * scale
    sq = raw_q * scale
    nv = mv[...] - STEP_SIZE * sv
    nq = mq[...] - STEP_SIZE * sq
    step_v[...] = sv
    step_q[...] = sq
    new_v[...] = nv
    new_q[...] = nq
    cop[me, :, :, 0:wv] = nv.astype(BF16).reshape(cparts, chalf, wv)
    cop[me, :, :, wv : wv + wq] = nq.astype(BF16).reshape(cparts, chalf, wq)
    copies = Gather(lambda index, p: cop.at[index, p], cparts, nz, nx, me, csend, crecv)
    copies.whole()
    copy_v[...] = cop[:, :, :, 0:wv].reshape(nfs * rows, wv)
    copy_q[...] = cop[:, :, :, wv : wv + wq].reshape(nfs * rows, wq)

    factors.drain()
    for p in range(fparts):
        for k in range(1, nfs):
            to_sibling(p, (me + k) % nfs).wait_send()
    everything.wait_send()
    told.wait_send()
    directions.drain()
    copies.drain()


def grid_of(n):
    nx = 1
    for d in range(1, n + 1):
        if n % d == 0 and d * d <= n:
            nx = d
    return n // nx, nx


def solution(mesh):
    nfs, ntp = mesh.shape["fs"], mesh.shape["tp"]
    nz, nx = grid_of(nfs)

    def step(x, cv, cq, mv, mq, fv, fq, v1, v2, q1, q2):
        tokens, depth = x.shape
        wv, wq = cv.shape[1], cq.shape[1]
        rows, rank = fv.shape
        rk = v1.shape[0]
        w = wv + wq
        blocks = 4
        width = depth // blocks
        two = lambda size, tile: 2 if size % (2 * tile) == 0 else 1
        fparts, dparts, cparts = two(rows, 16), two(rk, 8), two(rows, 16)
        kinds = 1 + nx
        dma = pltpu.SemaphoreType.DMA
        like = lambda shape, dtype: jax.ShapeDtypeStruct(shape, dtype)
        return pl.pallas_call(
            functools.partial(
                kernel, nfs, ntp, nz, nx, float(tokens * nfs), float(rank * w * ntp)
            ),
            out_shape=(
                like((rows, wv), F32), like((rows, wq), F32),
                like((rows, wv), F32), like((rows, wq), F32),
                like((depth, wv), BF16), like((depth, wq), BF16),
                like((rk, wv), F32), like((rk, wv), F32),
                like((rk, wq), F32), like((rk, wq), F32),
            ),
            in_specs=[pl.BlockSpec(memory_space=pl.ANY)] * 11,
            out_specs=tuple([pl.BlockSpec(memory_space=pltpu.VMEM)] * 10),
            scratch_shapes=[
                pltpu.VMEM((blocks, tokens, width), BF16),
                pltpu.VMEM((tokens, wv), BF16),
                pltpu.VMEM((tokens, wq), BF16),
                pltpu.VMEM((w, tokens), BF16),
                pltpu.VMEM((blocks, w, width), BF16),
                pltpu.VMEM((blocks, w, width), BF16),
                pltpu.VMEM((2, nfs, fparts, rows // fparts, rank), BF16),
                pltpu.VMEM((nfs, rk, w), F32),
                pltpu.VMEM((nfs - 1, rk, w), F32),
                pltpu.VMEM((nfs, dparts, rk // dparts, w), F32),
                pltpu.VMEM((nfs * ntp, 8, 128), F32),
                pltpu.VMEM((nfs, cparts, rows // cparts, w), BF16),
                pltpu.VMEM((rows, wv), F32),
                pltpu.VMEM((rows, wq), F32),
                pltpu.VMEM((rk, wv), F32),
                pltpu.VMEM((rk, wv), F32),
                pltpu.VMEM((rk, wq), F32),
                pltpu.VMEM((rk, wq), F32),
                dma((2 * fparts + 8,)),
                dma((blocks,)),
                dma((fparts, nfs, kinds)),
                dma((fparts, nfs)),
                dma((fparts, nfs)),
                dma((fparts, nfs)),
                dma((dparts, nfs, kinds)),
                dma((dparts, nfs)),
                dma((cparts, nfs, kinds)),
                dma((cparts, nfs)),
                dma((2,)),
                dma((2,)),
            ],
            compiler_params=pltpu.CompilerParams(
                collective_id=0, has_side_effects=True, vmem_limit_bytes=56 * 1024 * 1024
            ),
            name="moment_step",
        )(x, cv, cq, mv, mq, fv, fq, v1, v2, q1, q2)

    tall, both = P("fs", None), P("fs", "tp")
    return jax.shard_map(
        step,
        mesh=mesh,
        in_specs=(tall, both, both, both, both, tall, tall, both, both, both, both),
        out_specs=(both, both, both, both, P(None, "tp"), P(None, "tp"), both, both, both, both),
        check_vma=False,
    )
```

time: 376 us -> 94.7 us (0.25)
  waiting for transfers between devices: 197 us -> 0 us
  blocking collectives: 133 us -> 0 us
  Pallas kernels: 0 us -> 77.5 us
  matrix products: 19 us -> 0 us
  between operations: 15.9 us -> 0.66 us
  local copies, waits for them, and re-layouts: 6.72 us -> 16 us
  other arithmetic: 3.92 us -> 0 us
    reduce_scatter x2 -> x0, waiting for transfers between devices: 118 us -> none  [the longest x1 63 us: on_device(): lax.psum_scatter(value_part, 'fs', scatter_dimension=0, tiled=True)]
    all_gather x3 -> x0, blocking collectives: 93.2 us -> none  [the longest x1 31.5 us: on_device(): lax.all_gather(query_master_new.astype(jnp.bfloat16), 'fs', axis=0, tiled...]
    pallas_call x0 -> x1, Pallas kernels: none -> 77.5 us  [step(): pl.pallas_call(functools.partial(kernel, nfs, ntp, nz, nx, float(tokens *...]
    all_gather x3 -> x0, waiting for transfers between devices: 76.7 us -> none  [the longest x1 44.4 us: on_device(): lax.all_gather(query_factor, 'fs', axis=0, tiled=True)]
    psum x1 -> x0, blocking collectives: 40.1 us -> none  [on_device(): lax.psum(jnp.sum(value_dir_own * value_dir_own) + jnp.sum(query_dir_own *...]
    dot_general x6 -> x0, matrix products: 19 us -> none  [the longest x1 5.91 us: on_device(): jnp.dot(saved_input, lax.all_gather(query_factor, 'fs', axis=0, tiled=Tru...]
    unnamed x28 -> x10, local copies, waits for them, and re-layouts: 6.72 us -> 16 us
    reduce_sum x2 -> x0, other arithmetic: 3.92 us -> none  [the longest x1 1.99 us: on_device(): jnp.sum(value_dir_own * value_dir_own)]
  transfers between devices with their start and end apart: 5 -> 0, of which waited for: 4 -> 0; matrix products, arithmetic and copies ran while one was open for 6% -> 0% of each run, Pallas kernels for 0% -> 0%
where the time goes in v1:
time: 94.7 us; the launch traced here: 94.1 us
  Pallas kernels  77.5 us (82%)
  local copies, waits for them, and re-layouts  16 us (17%)
    pallas_call x1, Pallas kernels, step(): pl.pallas_call(functools.partial(kernel, nfs, ntp, nz, nx, float(tokens *...  77.5 us
    unnamed x10, local copies, waits for them, and re-layouts  16 us

profile of v1, /device:TPU:0, one launch (start us, length us, event | category | flops | bytes accessed | tf_op | source)
XLA Modules:
  0.0 94.1 jit_solution(5828608984299056227)
XLA Ops:
  0.6 77.5 %moment_step.1 = (f32[256,256]{1,0:T(8,128)}, f32[256,128]{1,0:T(8,128)}, f32[256,256]{1,0:T(8,128)}, f32[256,128]{1,0:T(8,128)}, bf16[2048,256]{1,0:T(8,128)(2,...) custom-call(bf16[2560,2048]{1,0:T(8,128)(2,1)} %x_in.1, ...), custom_call_target="tpu_custom_call" | custom-call | tf_op jit(solution)/shard_map/moment_step/pallas_call | solution.py:369
  78.1 1.7 %copy.31 = f32[256,256]{1,0:T(8,128)} copy(f32[256,256]{1,0:T(8,128)} %get-tuple-element.20) | data formatting | bytes 524288
  79.8 1.6 %copy.32 = f32[256,128]{1,0:T(8,128)} copy(f32[256,128]{1,0:T(8,128)} %get-tuple-element.21) | data formatting | bytes 262144
  81.4 1.7 %copy.33 = f32[256,256]{1,0:T(8,128)} copy(f32[256,256]{1,0:T(8,128)} %get-tuple-element.22) | data formatting | bytes 524288
  83.0 1.6 %copy.34 = f32[256,128]{1,0:T(8,128)} copy(f32[256,128]{1,0:T(8,128)} %get-tuple-element.23) | data formatting | bytes 262144
  84.6 2.3 %copy.35 = bf16[2048,256]{1,0:T(8,128)(2,1)} copy(bf16[2048,256]{1,0:T(8,128)(2,1)} %get-tuple-element.24) | data formatting | bytes 2097152
  86.9 1.9 %copy.36 = bf16[2048,128]{1,0:T(8,128)(2,1)} copy(bf16[2048,128]{1,0:T(8,128)(2,1)} %get-tuple-element.25) | data formatting | bytes 1048576
  88.7 1.4 %copy.37 = f32[32,256]{1,0:T(8,128)} copy(f32[32,256]{1,0:T(8,128)} %get-tuple-element.26) | data formatting | bytes 65536
  90.1 1.4 %copy.38 = f32[32,256]{1,0:T(8,128)} copy(f32[32,256]{1,0:T(8,128)} %get-tuple-element.27) | data formatting | bytes 65536
  91.5 1.3 %copy.39 = f32[32,128]{1,0:T(8,128)} copy(f32[32,128]{1,0:T(8,128)} %get-tuple-element.28) | data formatting | bytes 32768
  92.8 1.3 %copy.40 = f32[32,128]{1,0:T(8,128)} copy(f32[32,128]{1,0:T(8,128)} %get-tuple-element.29) | data formatting | bytes 32768

commit v2 on v1

--- a/solution.py
+++ b/solution.py
@@ -28,6 +28,7 @@
         self.me, self.z, self.x = me, me // nx, me % nx
         self.send_sem, self.recv_sem, self.extra = send_sem, recv_sem, extra
         self.sent = []
+        self.direct = max(parts - 1, 1)
 
     def copy(self, part, index, kind, peer):
         ref = self.slot(index, part)
@@ -72,43 +73,47 @@
 
     def start(self):
         yes = self.z >= 0
+        for part in range(self.direct, self.parts):
+            self.across(part, self.me, yes)
         for part in range(self.parts):
-            if part == 1:
-                self.across(part, self.me, yes)
             self.up(part, self.me, yes)
             self.down(part, self.me, yes)
-            if part == 0:
+            if part < self.direct:
                 self.across(part, self.me, yes)
 
     def side(self):
         yes = self.z >= 0
-        for k in range(1, self.nx):
-            index = self.z * self.nx + (self.x + k) % self.nx
-            if self.parts > 1:
-                self.arrived(1, index, yes)
-                self.up(1, index, yes)
-                self.down(1, index, yes)
+        for part in range(self.direct, self.parts):
+            for k in range(1, self.nx):
+                index = self.z * self.nx + (self.x + k) % self.nx
+                self.arrived(part, index, yes)
+                self.up(part, index, yes)
+                self.down(part, index, yes)
 
     def hop(self, s):
         below, above = self.z >= s, self.z + s < self.nz
         low = jnp.maximum(self.z - s, 0) * self.nx
         high = jnp.minimum(self.z + s, self.nz - 1) * self.nx
-        for where, base, onward in ((below, low, self.up), (above, high, self.down)):
-            index = base + self.x
-            self.arrived(0, index, where)
-            onward(0, index, where)
-            self.across(0, index, where)
-            if self.parts > 1:
-                for k in range(self.nx):
+        ways = ((below, low, self.up), (above, high, self.down))
+        for part in range(self.direct):
+            for where, base, onward in ways:
+                index = base + self.x
+                self.arrived(part, index, where)
+                onward(part, index, where)
+                self.across(part, index, where)
+        for part in range(self.direct, self.parts):
+            for k in range(self.nx):
+                for where, base, onward in ways:
                     index = base + (self.x + k) % self.nx
-                    self.arrived(1, index, where)
-                    onward(1, index, where)
+                    self.arrived(part, index, where)
+                    onward(part, index, where)
 
     def last(self):
         yes = self.z >= 0
-        for z in range(self.nz):
-            for k in range(1, self.nx):
-                self.arrived(0, z * self.nx + (self.x + k) % self.nx, yes)
+        for part in range(self.direct):
+            for z in range(self.nz):
+                for k in range(1, self.nx):
+                    self.arrived(part, z * self.nx + (self.x + k) % self.nx, yes)
 
     def drain(self):
         for where, done in self.sent:
@@ -161,20 +166,20 @@
         load(src, dst)
 
     barrier = pltpu.get_barrier_semaphore()
-    devices = nfs * ntp
-    mine = me * ntp + tp
-
-    def greet(k, _):
-        other = (mine + k) % devices
-        pl.semaphore_signal(
-            barrier, inc=1, device_id={"fs": other // ntp, "tp": other % ntp}, device_id_type=MESH
-        )
+
+    def greet_fs(k, _):
+        pl.semaphore_signal(barrier, inc=1, device_id={"fs": (me + k) % nfs}, device_id_type=MESH)
         return 0
 
-    lax.fori_loop(1, devices, greet, 0)
+    def greet_tp(k, _):
+        pl.semaphore_signal(barrier, inc=1, device_id={"tp": (tp + k) % ntp}, device_id_type=MESH)
+        return 0
+
+    lax.fori_loop(1, nfs, greet_fs, 0)
+    lax.fori_loop(1, ntp, greet_tp, 0)
     for copy in loads[:nfac]:
         copy.wait()
-    pl.semaphore_wait(barrier, devices - 1)
+    pl.semaphore_wait(barrier, nfs + ntp - 2)
 
     def to_sibling(p, index):
         return pltpu.make_async_remote_copy(
@@ -261,7 +266,6 @@
     for k in range(nfs - 1):
         share = share + landed[k]
 
-    square = jnp.zeros((), F32)
     for cols, first_ref, second_ref, first_out, second_out in (
         (slice(0, wv), m1v, m2v, v1, v2),
         (slice(wv, wv + wq), m1q, m2q, q1, q2),
@@ -273,31 +277,29 @@
         second_out[...] = second_new
         direction = first_new / (jnp.sqrt(second_new) + DENOM_EPS)
         dirs[me, :, :, cols] = direction.reshape(dparts, dhalf, direction.shape[1])
-        square = square + jnp.sum(direction * direction)
-    sums[devices - 1] = jnp.full(sums.shape[1:], square, F32)
 
     directions = Gather(lambda index, p: dirs.at[index, p], dparts, nz, nx, me, dsend, drecv)
     directions.start()
-
-    def tell(k, _):
-        other = (mine + k) % devices
-        pltpu.make_async_remote_copy(
-            src_ref=sums.at[devices - 1],
-            dst_ref=sums.at[devices - 1 - k],
-            send_sem=sum_sem.at[0],
-            recv_sem=sum_sem.at[1],
-            device_id={"fs": other // ntp, "tp": other % ntp},
-            device_id_type=MESH,
-        ).start()
-        return 0
-
-    lax.fori_loop(1, devices, tell, 0)
     directions.side()
     for s in range(1, nz):
         directions.hop(s)
     directions.last()
 
     full = dirs[...].reshape(rank, wv + wq)
+    sums[ntp - 1] = jnp.full(sums.shape[1:], jnp.sum(full * full), F32)
+
+    def tell(k, _):
+        pltpu.make_async_remote_copy(
+            src_ref=sums.at[ntp - 1],
+            dst_ref=sums.at[ntp - 1 - k],
+            send_sem=sum_sem.at[0],
+            recv_sem=sum_sem.at[1],
+            device_id={"tp": (tp + k) % ntp},
+            device_id_type=MESH,
+        ).start()
+        return 0
+
+    lax.fori_loop(1, ntp, tell, 0)
     high = full.astype(BF16)
     low = (full - high.astype(F32)).astype(BF16)
     own_v = fac[0, me].reshape(rows, rank)
@@ -306,8 +308,8 @@
     raw_q = split_dot(own_q, low[:, wv:]) + split_dot(own_q, high[:, wv:])
 
     told = pltpu.make_async_remote_copy(
-        src_ref=sums.at[pl.ds(0, devices - 1)],
-        dst_ref=sums.at[pl.ds(0, devices - 1)],
+        src_ref=sums.at[pl.ds(0, ntp - 1)],
+        dst_ref=sums.at[pl.ds(0, ntp - 1)],
         send_sem=sum_sem.at[0],
         recv_sem=sum_sem.at[1],
         device_id={"fs": me},
@@ -341,6 +343,15 @@
     copies.drain()
 
 
+def hand_over(*refs):
+    sem, count = refs[-1], len(refs) // 2
+    copies = [pltpu.make_async_copy(refs[i], refs[count + i], sem.at[i]) for i in range(count)]
+    for copy in copies:
+        copy.start()
+    for copy in copies:
+        copy.wait()
+
+
 def grid_of(n):
     nx = 1
     for d in range(1, n + 1):
@@ -361,12 +372,12 @@
         w = wv + wq
         blocks = 4
         width = depth // blocks
-        two = lambda size, tile: 2 if size % (2 * tile) == 0 else 1
-        fparts, dparts, cparts = two(rows, 16), two(rk, 8), two(rows, 16)
+        four = lambda size, tile: 4 if size % (4 * tile) == 0 else 1
+        fparts, dparts, cparts = four(rows, 16), 1, four(rows, 16)
         kinds = 1 + nx
         dma = pltpu.SemaphoreType.DMA
         like = lambda shape, dtype: jax.ShapeDtypeStruct(shape, dtype)
-        return pl.pallas_call(
+        outs = pl.pallas_call(
             functools.partial(
                 kernel, nfs, ntp, nz, nx, float(tokens * nfs), float(rank * w * ntp)
             ),
@@ -390,7 +401,7 @@
                 pltpu.VMEM((nfs, rk, w), F32),
                 pltpu.VMEM((nfs - 1, rk, w), F32),
                 pltpu.VMEM((nfs, dparts, rk // dparts, w), F32),
-                pltpu.VMEM((nfs * ntp, 8, 128), F32),
+                pltpu.VMEM((ntp, 8, 128), F32),
                 pltpu.VMEM((nfs, cparts, rows // cparts, w), BF16),
                 pltpu.VMEM((rows, wv), F32),
                 pltpu.VMEM((rows, wq), F32),
@@ -412,10 +423,19 @@
                 dma((2,)),
             ],
             compiler_params=pltpu.CompilerParams(
-                collective_id=0, has_side_effects=True, vmem_limit_bytes=56 * 1024 * 1024
+                collective_id=0, has_side_effects=True, vmem_limit_bytes=36 * 1024 * 1024
             ),
             name="moment_step",
         )(x, cv, cq, mv, mq, fv, fq, v1, v2, q1, q2)
+        return pl.pallas_call(
+            hand_over,
+            out_shape=tuple(like(o.shape, o.dtype) for o in outs),
+            in_specs=[pl.BlockSpec(memory_space=pltpu.VMEM)] * len(outs),
+            out_specs=tuple([pl.BlockSpec(memory_space=pl.ANY)] * len(outs)),
+            scratch_shapes=[dma((len(outs),))],
+            compiler_params=pltpu.CompilerParams(vmem_limit_bytes=8 * 1024 * 1024),
+            name="hand_over",
+        )(*outs)
 
     tall, both = P("fs", None), P("fs", "tp")
     return jax.shard_map(

time: 94.7 us -> 86.3 us (0.911)
  Pallas kernels: 77.5 us -> 72.1 us
  local copies, waits for them, and re-layouts: 16 us -> 13 us
    pallas_call x1, Pallas kernels: 77.5 us -> 70.6 us  [step(): pl.pallas_call(functools.partial(kernel, nfs, ntp, nz, nx, float(tokens *...]
    unnamed x10 -> x22, local copies, waits for them, and re-layouts: 16 us -> 13 us
    pallas_call x0 -> x1, Pallas kernels: none -> 1.5 us  [step(): pl.pallas_call(hand_over, out_shape=tuple((like(o.shape, o.dtype) for o i...]
where the time goes in v2:
time: 86.3 us; the launch traced here: 85.8 us
  Pallas kernels  72.1 us (84%)
  local copies, waits for them, and re-layouts  13 us (15%)
    pallas_call x1, Pallas kernels, step(): pl.pallas_call(functools.partial(kernel, nfs, ntp, nz, nx, float(tokens *...  70.6 us
    unnamed x22, local copies, waits for them, and re-layouts  13 us

profile of v2, /device:TPU:0, one launch (start us, length us, event | category | flops | bytes accessed | tf_op | source)
XLA Modules:
  0.0 85.8 jit_solution(1804656651640790868)
XLA Ops:
  0.6 0.0 copy-start
  0.7 4.0 %copy-done = bf16[2560,2048]{1,0:T(8,128)(2,1)S(1)} copy-done((bf16[2560,2048]{1,0:T(8,128)(2,1)S(1)}, bf16[2560,2048]{1,0:T(8,128)(2,1)}, u32[]{:S(2)}) %copy-start) | copy-done | bytes 10485784
  4.6 0.0 copy-start.1
  4.6 1.3 %copy-done.1 = bf16[2560,256]{1,0:T(8,128)(2,1)S(1)} copy-done((bf16[2560,256]{1,0:T(8,128)(2,1)S(1)}, bf16[2560,256]{1,0:T(8,128)(2,1)}, u32[]{:S(2)}) %copy-start.1) | copy-done | bytes 1310744
  5.9 0.0 copy-start.2
  5.9 1.1 %copy-done.2 = bf16[2560,128]{1,0:T(8,128)(2,1)S(1)} copy-done((bf16[2560,128]{1,0:T(8,128)(2,1)S(1)}, bf16[2560,128]{1,0:T(8,128)(2,1)}, u32[]{:S(2)}) %copy-start.2) | copy-done | bytes 655384
  7.0 0.0 copy-start.3
  7.0 0.9 %copy-done.3 = f32[256,256]{1,0:T(8,128)S(1)} copy-done((f32[256,256]{1,0:T(8,128)S(1)}, f32[256,256]{1,0:T(8,128)}, u32[]{:S(2)}) %copy-start.3) | copy-done | bytes 262168
  8.0 0.0 copy-start.4
  8.0 0.9 %copy-done.4 = f32[256,128]{1,0:T(8,128)S(1)} copy-done((f32[256,128]{1,0:T(8,128)S(1)}, f32[256,128]{1,0:T(8,128)}, u32[]{:S(2)}) %copy-start.4) | copy-done | bytes 131096
  8.9 0.0 copy-start.5
  8.9 0.9 %copy-done.5 = bf16[256,256]{1,0:T(8,128)(2,1)S(1)} copy-done((bf16[256,256]{1,0:T(8,128)(2,1)S(1)}, bf16[256,256]{1,0:T(8,128)(2,1)}, u32[]{:S(2)}) %copy-start.5) | copy-done | bytes 131096
  9.8 0.0 copy-start.6
  9.8 0.9 %copy-done.6 = bf16[256,256]{1,0:T(8,128)(2,1)S(1)} copy-done((bf16[256,256]{1,0:T(8,128)(2,1)S(1)}, bf16[256,256]{1,0:T(8,128)(2,1)}, u32[]{:S(2)}) %copy-start.6) | copy-done | bytes 131096
  10.7 0.0 copy-start.7
  10.7 0.8 copy-done.7
  11.5 0.0 copy-start.8
  11.5 0.8 copy-done.8
  12.2 0.0 copy-start.9
  12.2 0.7 copy-done.9
  12.9 0.0 copy-start.10
  12.9 0.7 copy-done.10
  13.6 70.6 %moment_step.1 = (f32[256,256]{1,0:T(8,128)S(1)}, f32[256,128]{1,0:T(8,128)S(1)}, f32[256,256]{1,0:T(8,128)S(1)}, f32[256,128]{1,0:T(8,128)S(1)}, bf16[2048,256]...) custom-call(bf16[2560,2048]{1,0:T(8,128)(2,1)S(1)} %copy-done, ...), custom_call_target="tpu_custom_call" | custom-call | tf_op jit(solution)/shard_map/moment_step/pallas_call | solution.py:380
  84.3 1.5 %hand_over.1 = (f32[256,256]{1,0:T(8,128)}, f32[256,128]{1,0:T(8,128)}, f32[256,256]{1,0:T(8,128)}, f32[256,128]{1,0:T(8,128)}, bf16[2048,256]{1,0:T(8,128)(2,1)...) custom-call(f32[256,256]{1,0:T(8,128)S(1)} %get-tuple-element.20.ref, ...), custom_call_target="tpu_custom_call" | custom-call | tf_op jit(solution)/shard_map/hand_over/pallas_call | solution.py:430
Async XLA Ops:
  0.6 4.0 %copy-start = (bf16[2560,2048]{1,0:T(8,128)(2,1)S(1)}, bf16[2560,2048]{1,0:T(8,128)(2,1)}, u32[]{:S(2)}) copy-start(bf16[2560,2048]{1,0:T(8,128)(2,1)} %x_in.1) | copy-start | bytes 31457284
  4.6 1.3 %copy-start.1 = (bf16[2560,256]{1,0:T(8,128)(2,1)S(1)}, bf16[2560,256]{1,0:T(8,128)(2,1)}, u32[]{:S(2)}) copy-start(bf16[2560,256]{1,0:T(8,128)(2,1)} %cv_in.1) | copy-start | bytes 3932164
  5.9 1.1 %copy-start.2 = (bf16[2560,128]{1,0:T(8,128)(2,1)S(1)}, bf16[2560,128]{1,0:T(8,128)(2,1)}, u32[]{:S(2)}) copy-start(bf16[2560,128]{1,0:T(8,128)(2,1)} %cq_in.1) | copy-start | bytes 1966084
  7.0 0.9 %copy-start.3 = (f32[256,256]{1,0:T(8,128)S(1)}, f32[256,256]{1,0:T(8,128)}, u32[]{:S(2)}) copy-start(f32[256,256]{1,0:T(8,128)} %mv_in.1) | copy-start | bytes 786436
  8.0 0.9 %copy-start.4 = (f32[256,128]{1,0:T(8,128)S(1)}, f32[256,128]{1,0:T(8,128)}, u32[]{:S(2)}) copy-start(f32[256,128]{1,0:T(8,128)} %mq_in.1) | copy-start | bytes 393220
  8.9 0.9 %copy-start.5 = (bf16[256,256]{1,0:T(8,128)(2,1)S(1)}, bf16[256,256]{1,0:T(8,128)(2,1)}, u32[]{:S(2)}) copy-start(bf16[256,256]{1,0:T(8,128)(2,1)} %fv_in.1) | copy-start | bytes 393220
  9.8 0.9 %copy-start.6 = (bf16[256,256]{1,0:T(8,128)(2,1)S(1)}, bf16[256,256]{1,0:T(8,128)(2,1)}, u32[]{:S(2)}) copy-start(bf16[256,256]{1,0:T(8,128)(2,1)} %fq_in.1) | copy-start | bytes 393220
  10.7 0.8 copy-start.7
  11.5 0.8 copy-start.8
  12.2 0.7 copy-start.9
  12.9 0.7 copy-start.10

commit v3 on v2

--- a/solution.py
+++ b/solution.py
@@ -344,12 +344,17 @@
 
 
 def hand_over(*refs):
-    sem, count = refs[-1], len(refs) // 2
-    copies = [pltpu.make_async_copy(refs[i], refs[count + i], sem.at[i]) for i in range(count)]
-    for copy in copies:
-        copy.start()
-    for copy in copies:
-        copy.wait()
+    sem, count = refs[-1], len(refs) // 3
+    source, result, held = refs[:count], refs[count : 2 * count], refs[2 * count : 3 * count]
+    takes = [pltpu.make_async_copy(source[i], held[i], sem.at[0, i]) for i in range(count)]
+    gives = [pltpu.make_async_copy(held[i], result[i], sem.at[1, i]) for i in range(count)]
+    for take in takes:
+        take.start()
+    for take, give in zip(takes, gives):
+        take.wait()
+        give.start()
+    for give in gives:
+        give.wait()
 
 
 def grid_of(n):
@@ -388,7 +393,7 @@
                 like((rk, wv), F32), like((rk, wv), F32),
                 like((rk, wq), F32), like((rk, wq), F32),
             ),
-            in_specs=[pl.BlockSpec(memory_space=pl.ANY)] * 11,
+            in_specs=[pl.BlockSpec(memory_space=pltpu.HBM)] * 11,
             out_specs=tuple([pl.BlockSpec(memory_space=pltpu.VMEM)] * 10),
             scratch_shapes=[
                 pltpu.VMEM((blocks, tokens, width), BF16),
@@ -423,17 +428,17 @@
                 dma((2,)),
             ],
             compiler_params=pltpu.CompilerParams(
-                collective_id=0, has_side_effects=True, vmem_limit_bytes=36 * 1024 * 1024
+                collective_id=0, has_side_effects=True, vmem_limit_bytes=60 * 1024 * 1024
             ),
             name="moment_step",
         )(x, cv, cq, mv, mq, fv, fq, v1, v2, q1, q2)
         return pl.pallas_call(
             hand_over,
             out_shape=tuple(like(o.shape, o.dtype) for o in outs),
-            in_specs=[pl.BlockSpec(memory_space=pltpu.VMEM)] * len(outs),
+            in_specs=[pl.BlockSpec(memory_space=pl.ANY)] * len(outs),
             out_specs=tuple([pl.BlockSpec(memory_space=pl.ANY)] * len(outs)),
-            scratch_shapes=[dma((len(outs),))],
-            compiler_params=pltpu.CompilerParams(vmem_limit_bytes=8 * 1024 * 1024),
+            scratch_shapes=[pltpu.VMEM(o.shape, o.dtype) for o in outs] + [dma((2, len(outs)))],
+            compiler_params=pltpu.CompilerParams(vmem_limit_bytes=60 * 1024 * 1024),
             name="hand_over",
         )(*outs)
 

time: 86.3 us -> 73.1 us (0.85)
  local copies, waits for them, and re-layouts: 13 us -> 0 us
    unnamed x22 -> x0, local copies, waits for them, and re-layouts: 13 us -> none
    pallas_call x1, Pallas kernels: 1.5 us -> 2.83 us  [step(): pl.pallas_call(hand_over, out_shape=tuple((like(o.shape, o.dtype) for o i...]
    pallas_call x1, Pallas kernels: 70.6 us -> 69.5 us  [step(): pl.pallas_call(functools.partial(kernel, nfs, ntp, nz, nx, float(tokens *...]
where the time goes in v3:
time: 73.1 us; the launch traced here: 73 us
  Pallas kernels  72.3 us (99%)
    pallas_call x1, Pallas kernels, step(): pl.pallas_call(functools.partial(kernel, nfs, ntp, nz, nx, float(tokens *...  69.5 us
    pallas_call x1, Pallas kernels, step(): pl.pallas_call(hand_over, out_shape=tuple((like(o.shape, o.dtype) for o i...  2.83 us

profile of v3, /device:TPU:0, one launch (start us, length us, event | category | flops | bytes accessed | tf_op | source)
XLA Modules:
  0.0 73.0 jit_solution(18224147492693752406)
XLA Ops:
  0.6 69.5 %moment_step.1 = (f32[256,256]{1,0:T(8,128)}, f32[256,128]{1,0:T(8,128)}, f32[256,256]{1,0:T(8,128)}, f32[256,128]{1,0:T(8,128)}, bf16[2048,256]{1,0:T(8,128)(2,...) custom-call(bf16[2560,2048]{1,0:T(8,128)(2,1)} %x_in.1, ...), custom_call_target="tpu_custom_call" | custom-call | tf_op jit(solution)/shard_map/moment_step/pallas_call | solution.py:385
  70.2 2.8 %hand_over.1 = (f32[256,256]{1,0:T(8,128)}, f32[256,128]{1,0:T(8,128)}, f32[256,256]{1,0:T(8,128)}, f32[256,128]{1,0:T(8,128)}, bf16[2048,256]{1,0:T(8,128)(2,1)...) custom-call(f32[256,256]{1,0:T(8,128)} %get-tuple-element.20.refs_0_, ...), custom_call_target="tpu_custom_call" | custom-call | tf_op jit(solution)/shard_map/hand_over/pallas_call | solution.py:435
